TPU v7x, 256 devices: a whole 4x4x8 slice. The times are simulated.
256 devices in a mesh: ep: 64 (over z, y, core), tp: 4 (over x).
Axes of the slice: x: 4, y: 4, z: 8, core: 2. Of those that a mesh axis runs over, the one named last changes fastest.
Arguments:
- queries: bfloat16 [16384, 8, 128], P('ep', 'tp'), may hold values from -15 to 15
- keys: bfloat16 [16384, 4, 128], P('ep', 'tp'), may hold values from -6 to 6
- values: bfloat16 [16384, 4, 128], P('ep', 'tp'), may hold values from -6 to 6
- key_bias: bfloat16 [16384, 8], P('ep', 'tp'), may hold values from -20 to 2
- out_weight: bfloat16 [1024, 2048], P('tp'), may hold values from -0.1875 to 0.1875
- tokens_b: bfloat16 [32768, 2048], P(('ep', 'tp')), may hold values from -6 to 6
- moe_gain: bfloat16 [2048], replicated, may hold values from 0.099609375 to 1.8984375
- gate_weight: bfloat16 [64, 2048, 2048], P('ep', None, 'tp'), may hold values from -0.125 to 0.125
- up_weight: bfloat16 [64, 2048, 2048], P('ep', None, 'tp'), may hold values from -0.125 to 0.125
- down_weight: bfloat16 [64, 2048, 2048], P('ep', 'tp'), may hold values from -0.125 to 0.125
- routes: int32 [32768, 2], P(('ep', 'tp')), may hold values from 0 to 63, all different within a row; in each aligned block of 128 rows (0 to 127, 128 to 255, ...) at most 6 rows name the same one
- route_weights: float32 [32768, 2], P(('ep', 'tp')), may hold values from 0.2 to 1
Outputs:
- mixed: bfloat16 [16384, 2048], P(('ep', 'tp'))
- moe_out: bfloat16 [32768, 2048], P(('ep', 'tp'))
Inputs may be any that keep to these rules, and one draw needn't show every extreme that they name: `routes`: each row names 2 different experts. In each aligned block of 128 rows (the rows of one device) no expert is named by more than 6 rows, and in some block one expert is named by exactly 6 rows.
All inputs are finite; a program needn't handle non-finite values.
Results may differ from a plain program's by a relative error of at most 0.012.
Values may be sent and summed in bfloat16 or wider, within the bound.
A program may use at most 128 MiB of HBM per device.

v0:
```python
import math
import jax
import jax.numpy as jnp
from jax import lax
from jax.sharding import PartitionSpec as P


def in_one_piece(arrays, axis, dim, along):
    columns = [a.reshape(*a.shape[:along], -1) for a in arrays]
    both = jnp.concatenate(columns, axis=along)
    filled, at, done = (lax.all_gather(both, axis, axis=dim, tiled=True), 0, [])
    for a, column in zip(arrays, columns):
        share = filled[..., at : at + column.shape[along]]
        done.append(share.reshape(*share.shape[:along], *a.shape[along:]))
        at += column.shape[along]
    return tuple(done)


def partner(value, axis, apart):
    mask = 2**apart
    pairs = [(source, source ^ mask) for source in range(lax.axis_size(axis))]
    return lax.ppermute(value, axis, pairs)


def split_up(value, dim, length):
    before, after = (value.shape[:dim], value.shape[dim + 1 :])
    return jnp.moveaxis(value.reshape(*before, length, -1, *after), dim, 0)


def summed_on_arrival(value, axis, dim):
    pieces = split_up(value, dim, lax.axis_size(axis))
    arrived = lax.all_to_all(pieces, axis, split_axis=0, concat_axis=0, tiled=True)
    return arrived.astype(jnp.float32).sum(axis=0)


def entry_slots(routes, expert_total):
    flattened_expert_list = routes.reshape(-1)
    onehot = (
        flattened_expert_list[:, None] == jnp.arange(expert_total, dtype=jnp.int32)[None, :]
    ).astype(jnp.int32)
    earlier_count = jnp.cumsum(onehot, axis=0) - onehot
    return (flattened_expert_list, jnp.sum(earlier_count * onehot, axis=1))


def swiglu_rows(piece, gate_cols, up_cols):
    gate_val = jnp.dot(piece, gate_cols, preferred_element_type=jnp.float32)
    up_val = jnp.dot(piece, up_cols, preferred_element_type=jnp.float32)
    return (jax.nn.silu(gate_val) * up_val).astype(jnp.bfloat16)


def attend_rows(query_block, first_pos, keys_all, values_all, bias_all, local_kv):
    row_count, local_heads, head_dim = query_block.shape
    group_size = local_heads // local_kv
    key_total = keys_all.shape[0]
    key_span = min(1024, key_total)
    query_pos = first_pos + jnp.arange(row_count, dtype=jnp.int32)
    query_rows = query_block.reshape(row_count, local_kv, group_size, head_dim)
    visit_total = (first_pos + row_count + key_span - 1) // key_span
    score_scale = 1.0 / math.sqrt(head_dim)

    def visit(visit_no, state):
        accum, carried = state
        begin_at = (visit_total - 1 - visit_no) * key_span
        key_tile_rows = lax.dynamic_slice_in_dim(keys_all, begin_at, key_span, 0)
        value_block = lax.dynamic_slice_in_dim(values_all, begin_at, key_span, 0)
        bias_block = (
            lax.dynamic_slice_in_dim(bias_all, begin_at, key_span, 0)
            .astype(jnp.float32)
            .reshape(key_span, local_kv, group_size)
        )
        scores = (
            jnp.einsum(
                "rkgd,skd->kgrs", query_rows, key_tile_rows, preferred_element_type=jnp.float32
            )
            * score_scale
        )
        scores = scores + jnp.transpose(bias_block, (1, 2, 0))[:, :, None, :]
        key_pos = begin_at + jnp.arange(key_span, dtype=jnp.int32)
        earlier = key_pos[None, :] < query_pos[:, None]
        log_keep = jnp.where(earlier, jax.nn.log_sigmoid(-scores), 0.0)
        after = lax.cumsum(log_keep, axis=3, reverse=True) - log_keep
        weights = jnp.where(
            earlier, jnp.exp(jax.nn.log_sigmoid(scores) + after + carried[..., None]), 0.0
        ).astype(jnp.bfloat16)
        accum = accum + jnp.einsum(
            "kgrs,skd->kgrd", weights, value_block, preferred_element_type=jnp.float32
        )
        return (accum, carried + jnp.sum(log_keep, axis=3))

    start_state = (
        jnp.zeros((local_kv, group_size, row_count, head_dim), jnp.float32),
        jnp.zeros((local_kv, group_size, row_count), jnp.float32),
    )
    accum = lax.fori_loop(0, visit_total, visit, start_state)[0]
    return (
        jnp.transpose(accum, (2, 0, 1, 3))
        .reshape(row_count, local_heads * head_dim)
        .astype(jnp.bfloat16)
    )


def body(
    queries,
    keys,
    values,
    key_bias,
    out_weight,
    tokens_b,
    moe_gain,
    gate_weight,
    up_weight,
    down_weight,
    routes,
    route_weights,
):
    tok_rows, local_heads, head_dim = queries.shape
    local_kv = keys.shape[1]
    ep_count = lax.axis_size("ep")
    keys_all, values_all, bias_all = in_one_piece((keys, values, key_bias), "ep", 0, 1)
    device_ep = lax.axis_index("ep")
    half_rows = tok_rows // 2
    bit_count = ep_count.bit_length() - 1
    handed = queries[half_rows:]
    for bit_no in range(bit_count):
        handed = partner(handed, "ep", bit_no)
    companion_batch = ep_count - 1 - device_ep
    own_part = attend_rows(
        queries[:half_rows], device_ep * tok_rows, keys_all, values_all, bias_all, local_kv
    )
    other_part = attend_rows(
        handed, companion_batch * tok_rows + half_rows, keys_all, values_all, bias_all, local_kv
    )
    for bit_no in range(bit_count):
        other_part = partner(other_part, "ep", bit_no)
    attended = jnp.concatenate((own_part, other_part), axis=0)
    tok_b, model_width = tokens_b.shape
    top_count = routes.shape[1]
    expert_total = ep_count * gate_weight.shape[0]
    capacity = max(2, 3 * top_count * tok_b // (2 * expert_total))
    tokens_f = tokens_b.astype(jnp.float32)
    normed = (
        tokens_f
        * lax.rsqrt(jnp.mean(tokens_f * tokens_f, axis=1, keepdims=True) + 1e-06)
        * moe_gain.astype(jnp.float32)
    ).astype(jnp.bfloat16)
    flattened_expert_list, slot_index = entry_slots(routes, expert_total)
    place = flattened_expert_list * capacity + slot_index
    outbound = (
        jnp.zeros((expert_total * capacity, model_width), jnp.bfloat16)
        .at[place]
        .set(jnp.repeat(normed, top_count, axis=0))
    )
    outbound = outbound.reshape(expert_total, capacity, model_width)
    gate_cols = gate_weight[0]
    up_cols = up_weight[0]
    down_rows = down_weight[0]
    arrived = lax.all_to_all(outbound, "ep", split_axis=0, concat_axis=0, tiled=True)
    hidden = swiglu_rows(
        lax.all_gather(arrived.reshape(ep_count * capacity, model_width), "tp", axis=0, tiled=True),
        gate_cols,
        up_cols,
    )
    mixed_sum = lax.psum_scatter(
        jnp.dot(attended, out_weight, preferred_element_type=jnp.float32).astype(jnp.bfloat16),
        "tp",
        scatter_dimension=0,
        tiled=True,
    )
    expert_sum = summed_on_arrival(
        jnp.dot(hidden, down_rows, preferred_element_type=jnp.float32).astype(jnp.bfloat16), "tp", 0
    )
    returned = lax.all_to_all(
        expert_sum.astype(jnp.bfloat16).reshape(ep_count, capacity, model_width),
        "ep",
        split_axis=0,
        concat_axis=0,
        tiled=True,
    )
    picked = jnp.take(returned.reshape(expert_total * capacity, model_width), place, axis=0).astype(
        jnp.float32
    )
    weighted = picked * route_weights.reshape(-1)[:, None]
    moe_out = jnp.sum(weighted.reshape(tok_b, top_count, model_width), axis=1).astype(jnp.bfloat16)
    return (mixed_sum, moe_out)


def solution(mesh):
    in_specs = (
        P("ep", "tp", None),
        P("ep", "tp", None),
        P("ep", "tp", None),
        P("ep", "tp"),
        P("tp", None),
        P(("ep", "tp"), None),
        P(),
        P("ep", None, "tp"),
        P("ep", None, "tp"),
        P("ep", "tp", None),
        P(("ep", "tp"), None),
        P(("ep", "tp"), None),
    )
    out_specs = (P(("ep", "tp"), None), P(("ep", "tp"), None))
    return jax.shard_map(body, mesh=mesh, in_specs=in_specs, out_specs=out_specs, check_vma=False)
```

profile of v0, /device:TPU:8, one launch (start us, length us, event | category | flops | bytes accessed | tf_op | source)
XLA Modules:
  0.0 583.5 jit_solution(1064137814376958959)
XLA Ops:
  15.4 4.1 scatter_custom_fusion
  19.5 3.7 reshape.326
  23.2 63.4 %all_to_all.15 = bf16[64,6,2048]{2,1,0:T(8,128)(2,1)} all-to-all(bf16[64,6,2048]{2,1,0:T(8,128)(2,1)} %reshape.326), channel_id=1, replica_groups=mesh['ep'=64,'tp'=4] {'ep'}, dimensions={0} | all-to-all | bytes 3145728 | tf_op jit(solution)/shard_map/all_to_all | solution.py:157
  86.7 3.8 reshape.327
  93.4 3.7 collective-permute-done.1
  97.1 2.1 collective-permute-start.2
  99.2 3.7 collective-permute-done.2
  103.5 3.6 collective-permute-done.3
  107.3 5.1 collective-permute-done.4
  113.9 41.0 %all-gather.5.cloned.1.call-done = bf16[1536,2048]{1,0:T(8,128)(2,1)} async-done(((bf16[384,2048]{1,0:T(8,128)(2,1)}), bf16[1536,2048]{1,0:T(8,128)(2,1)}) %all-gather.5.cloned.1.call-update) | async-done | bytes 6291472 | tf_op jit(solution)/shard_map/all_gather | solution.py:159
  155.0 8.6 %fusion.53 = f32[1536,512]{1,0:T(8,128)} fusion(bf16[1536,2048]{1,0:T(8,128)(2,1)} %all-gather.5.cloned.1.call-done, bf16[1,2048,512]{2,1,0:T(8,128)(2,1)} %param.23), kind=kOutput, calls=%fused_computation.82 | convolution fusion | flops 3221225472 | bytes 11534336 | tf_op jit(solution)/shard_map/dot_general | solution.py:46
  163.6 11.8 %convolution_convert_fusion = bf16[1536,2048]{1,0:T(8,128)(2,1)} fusion(bf16[1,512,2048]{2,1,0:T(8,128)(2,1)S(1)} %copy-done, bf16[1536,2048]{1,0:T(8,128)(2,1)} %all-gather.5.cloned.1.call-done, f32[1536,512]{1,0:T(8,128)} %fusion.53, bf16[1,2048,512]{2,1,0:T(8,128)(2,1)} %param.24), kind=kOutput, calls=%fused_computation.74 | convolution fusion | flops 6450315264 | bytes 19922944 | tf_op jit(solution)/shard_map/dot_general | solution.py:170
  175.3 5.3 all-to-all-start.1
  180.6 66.6 %all-gather.3.cloned.1.call-done = bf16[16384,258]{1,0:T(8,128)(2,1)} async-done(((bf16[256,258]{1,0:T(8,128)(2,1)}), bf16[16384,258]{1,0:T(8,128)(2,1)}) %all-gather.3.cloned.1.call-update) | async-done | bytes 8454160 | tf_op jit(solution)/shard_map/all_gather | solution.py:11
  247.2 5.7 slice_bitcast_fusion.4
  252.9 3.8 slice.59
  256.7 3.7 copy.53
  260.5 125.5 %while.31 = (s32[]{:T(128)}, f32[1,2,128,128]{3,2,1,0:T(8,128)S(1)}, f32[1,2,128]{2,1,0:T(2,128)S(1)}, s32[]{:T(128)}, s32[]{:T(128)}, /*index=5*/bf16[16384,1,1...) while((s32[]{:T(128)}, ...), condition=%wide.region_9.10_spmd.clone, body=%wide.region_5.9_spmd.clone.sunk | while | flops 176343936 | bytes 10775775 | solution.py:94
  260.8 1.9 fusion.99
  262.7 2.5 fusion.100
  268.6 1.9 fusion.99
  270.5 2.5 fusion.100
  276.5 1.9 fusion.99
  278.4 2.5 fusion.100
  284.3 1.9 fusion.99
  286.2 2.5 fusion.100
  292.2 1.9 fusion.99
  294.1 2.5 fusion.100
  300.0 1.9 fusion.99
  301.9 2.5 fusion.100
  307.8 1.9 fusion.99
  309.7 2.5 fusion.100
  315.7 1.9 fusion.99
  317.6 2.5 fusion.100
  323.5 1.9 fusion.99
  325.4 2.5 fusion.100
  331.4 1.9 fusion.99
  333.3 2.5 fusion.100
  339.2 1.9 fusion.99
  341.1 2.5 fusion.100
  347.1 1.9 fusion.99
  349.0 2.5 fusion.100
  354.9 1.9 fusion.99
  356.8 2.5 fusion.100
  362.7 1.9 fusion.99
  364.6 2.5 fusion.100
  370.6 1.9 fusion.99
  372.5 2.5 fusion.100
  380.3 2.5 fusion.100
  387.5 2.0 collective-permute-start.7
  389.4 2.5 collective-permute-done.7
  391.9 5.8 collective-permute-done.8
  397.7 4.3 collective-permute-done.9
  402.0 5.3 collective-permute-done.10
  407.3 4.2 reduce_sum.69
  413.1 10.0 %all-to-all-start.2 = ((bf16[64,6,2048]{2,1,0:T(8,128)(2,1)}), bf16[64,6,2048]{2,1,0:T(8,128)(2,1)}, u32[]{:S(2)}, u32[]{:S(2)}) async-start(bf16[64,6,2048]{2,1,0:T(8,128)(2,1)} %reshape.329), calls=%async_computation.3 | async-start | bytes 4194304 | tf_op jit(solution)/shard_map/all_to_all | solution.py:172
  423.2 8.1 %while.30 = (s32[]{:T(128)}, f32[1,2,128,128]{3,2,1,0:T(8,128)S(1)}, f32[1,2,128]{2,1,0:T(2,128)S(1)}, s32[]{:T(128)}, s32[]{:T(128)}, /*index=5*/bf16[16384,1,1...) while((s32[]{:T(128)}, ...), condition=%wide.region_4.5_spmd.clone, body=%wide.region_0.4_spmd.clone.sunk | while | flops 176343936 | bytes 10775775 | solution.py:94
  425.4 2.5 fusion.93
  431.4 2.7 convolution_convert_fusion.1
  434.6 39.7 %all-to-all-done.2 = bf16[64,6,2048]{2,1,0:T(8,128)(2,1)} async-done(((bf16[64,6,2048]{2,1,0:T(8,128)(2,1)}), bf16[64,6,2048]{2,1,0:T(8,128)(2,1)}, u32[]{:S(2)}, u32[]{:S(2)}) %all-to-all-start.2) | async-done | bytes 1572896 | tf_op jit(solution)/shard_map/all_to_all | solution.py:172
  474.3 3.7 reshape.330
  478.0 4.1 gather_fusion
  483.6 6.2 %multiply_reduce_fusion = bf16[128,2048]{1,0:T(8,128)(2,1)} fusion(bf16[128,2,2048]{2,1,0:T(2,128)(2,1)} %gather.7, pred[128,2]{1,0:T(8,128)(4,1)S(1)} %copy.62, f32[128,2]{1,0:T(8,128)S(1)} %copy.64), kind=kLoop, calls=%fused_computation.84 | loop fusion | flops 1835008 | bytes 1574144 | tf_op jit(solution)/shard_map/reduce_sum | solution.py:183
  489.9 86.8 %reduce-scatter.2.cloned.1.call-done = bf16[64,2048]{1,0:T(8,128)(2,1)} async-done(((bf16[256,2048]{1,0:T(8,128)(2,1)}), bf16[64,2048]{1,0:T(8,128)(2,1)}) %reduce-scatter.2.cloned.1.call-update) | async-done | bytes 262160 | tf_op jit(solution)/shard_map/reduce_scatter | solution.py:163
  (264 shorter events, 78.7 us)
Async XLA Ops:
  7.2 156.4 %copy-start = (bf16[1,512,2048]{2,1,0:T(8,128)(2,1)S(1)}, bf16[1,512,2048]{2,1,0:T(8,128)(2,1)}, u32[]{:S(2)}) copy-start(bf16[1,512,2048]{2,1,0:T(8,128)(2,1)} %param.25) | copy-start | bytes 6291460
  7.2 147.8 %all-gather.5.cloned.1.call-start = ((), (), s32[]{:S(2)}) async-start(), calls=%async_computation.6 | async-start | bytes 7864320 | tf_op jit(solution)/shard_map/all_gather | solution.py:159
  86.6 3.8 copy-start.6
  86.7 4.0 copy-start.3
  86.7 4.0 copy-start.4
  86.7 4.7 copy-start.2
  90.4 156.8 %all-gather.3.cloned.1.call-start = ((), (), s32[]{:S(2)}) async-start(), calls=%async_computation.4 | async-start | bytes 12779520 | tf_op jit(solution)/shard_map/all_gather | solution.py:11
  91.5 1.3 collective-permute-start
  92.9 4.3 collective-permute-start.1
  97.1 5.8 collective-permute-start.2
  102.9 4.3 collective-permute-start.3
  107.2 5.2 collective-permute-start.4
  112.4 148.1 %collective-permute-start.5 = (bf16[128,2,128]{2,0,1:T(8,128)(2,1)S(1)}, bf16[128,2,128]{2,0,1:T(8,128)(2,1)S(1)}, u32[]{:S(2)}, u32[]{:S(2)}) collective-permute-start(bf16[128,2,128]{2,0,1:T(8,128)(2,1)S(1)} %collective-permute-done.4), channel_id=1, source_target_pairs={{0,128},{4,132},{8,136},{12,140},{16,144},{20,148},{24,152},{28,15... | collective-permute-start | bytes 196616 | tf_op jit(solution)/shard_map/ppermute | solution.py:22
  175.3 232.0 %all-to-all-start.1 = ((bf16[4,384,2048]{2,1,0:T(8,128)(2,1)}), bf16[4,384,2048]{2,1,0:T(8,128)(2,1)}, u32[]{:S(2)}, u32[]{:S(2)}) async-start(bf16[4,384,2048]{2,1,0:T(8,128)(2,1)} %bitcast.212), calls=%async_computation.2 | async-start | bytes 12582912 | tf_op jit(solution)/shard_map/all_to_all | solution.py:32
  386.1 1.3 collective-permute-start.6
  387.5 4.5 collective-permute-start.7
  391.9 5.8 collective-permute-start.8
  397.7 4.3 collective-permute-start.9
  402.0 5.3 collective-permute-start.10
  407.3 24.1 %collective-permute-start.11 = (bf16[128,256]{0,1:T(8,128)(2,1)S(1)}, bf16[128,256]{0,1:T(8,128)(2,1)S(1)}, u32[]{:S(2)}, u32[]{:S(2)}) collective-permute-start(bf16[128,256]{0,1:T(8,128)(2,1)S(1)} %collective-permute-done.10), channel_id=1, source_target_pairs={{0,128},{4,132},{8,136},{12,140},{16,144},{20,148},{24,152},{28,15... | collective-permute-start | bytes 196616 | tf_op jit(solution)/shard_map/ppermute | solution.py:22
  413.1 61.2 %all-to-all-start.2 = ((bf16[64,6,2048]{2,1,0:T(8,128)(2,1)}), bf16[64,6,2048]{2,1,0:T(8,128)(2,1)}, u32[]{:S(2)}, u32[]{:S(2)}) async-start(bf16[64,6,2048]{2,1,0:T(8,128)(2,1)} %reshape.329), calls=%async_computation.3 | async-start | bytes 4194304 | tf_op jit(solution)/shard_map/all_to_all | solution.py:172
  423.1 153.6 %reduce-scatter.2.cloned.1.call-start = ((), (), s32[]{:S(2)}) async-start(), calls=%async_computation.5 | async-start | bytes 1310720 | tf_op jit(solution)/shard_map/reduce_scatter | solution.py:163
  431.3 3.0 copy-start.5
  431.3 3.2 copy-start.7
  478.0 98.7 %copy-start.1 = (bf16[1,512,2048]{2,1,0:T(8,128)(2,1)S(1)}, bf16[1,512,2048]{2,1,0:T(8,128)(2,1)}, u32[]{:S(2)}) copy-start(bf16[1,512,2048]{2,1,0:T(8,128)(2,1)} %param.25) | copy-start | bytes 6291460
Sparse Core Ops, SparseCore 0:
  90.6 64.3 all-gather.4
  158.3 88.9 all-gather.2
  434.2 142.4 reduce-scatter.1
where the time goes:
time: 592 us; the launch traced here: 583 us
  waiting for transfers between devices  270 us (46%)
  other arithmetic  89.5 us (15%)
  matrix products  77.4 us (13%)
  blocking collectives  63.4 us (11%)
  local copies, waits for them, and re-layouts  43.9 us (7%)
  starting transfers between devices  22.8 us (4%)
  between operations  14.2 us (2%)
    reduce_scatter x1, waiting for transfers between devices, body(): lax.psum_scatter(jnp.dot(attended, out_weight, preferred_element_type=jnp...  86.8 us
    all_gather x1, waiting for transfers between devices, in_one_piece(): filled, at, done = (lax.all_gather(both, axis, axis=dim, tiled=True), 0, [])  66.6 us
    all_to_all x1, blocking collectives, body(): lax.all_to_all(outbound, 'ep', split_axis=0, concat_axis=0, tiled=True)  63.4 us
    another operation x36, other arithmetic  44.3 us
    all_gather x1, waiting for transfers between devices, body(): lax.all_gather(arrived.reshape(ep_count * capacity, model_width), 'tp', a...  41 us
    all_to_all x1, waiting for transfers between devices, body(): lax.all_to_all(expert_sum.astype(jnp.bfloat16).reshape(ep_count, capacity...  39.7 us
    ppermute x12, waiting for transfers between devices, partner(): return lax.ppermute(value, axis, pairs)  36.2 us
    dot_general x17, matrix products, visit(): jnp.einsum('rkgd,skd->kgrs', query_rows, key_tile_rows, preferred_element...  32.2 us
  transfers between devices with their start and end apart: 17, of which 14 were waited for; matrix products, arithmetic and copies ran while one was open for 33% of the time, Pallas kernels for 0%

commit v1 on v0

--- a/solution.py
+++ b/solution.py
@@ -3,6 +3,25 @@
 import jax.numpy as jnp
 from jax import lax
 from jax.sharding import PartitionSpec as P
+
+
+def ring_gather(x, axis, dim):
+    size, index, span = (lax.axis_size(axis), lax.axis_index(axis), x.shape[dim])
+    forward = [(i, (i + 1) % size) for i in range(size)]
+    downward = [(i, (i - 1) % size) for i in range(size)]
+    out = jnp.zeros((*x.shape[:dim], size * span, *x.shape[dim + 1 :]), x.dtype)
+    out = lax.dynamic_update_slice_in_dim(out, x, index * span, axis=dim)
+    from_left = from_right = x
+    half = size // 2
+    for lap in range(1, half + 1):
+        from_left = lax.ppermute(from_left, axis, forward)
+        out = lax.dynamic_update_slice_in_dim(out, from_left, (index - lap) % size * span, axis=dim)
+        if lap < size - half:
+            from_right = lax.ppermute(from_right, axis, downward)
+            out = lax.dynamic_update_slice_in_dim(
+                out, from_right, (index + lap) % size * span, axis=dim
+            )
+    return out
 
 
 def in_one_piece(arrays, axis, dim, along):
@@ -156,9 +175,7 @@
     down_rows = down_weight[0]
     arrived = lax.all_to_all(outbound, "ep", split_axis=0, concat_axis=0, tiled=True)
     hidden = swiglu_rows(
-        lax.all_gather(arrived.reshape(ep_count * capacity, model_width), "tp", axis=0, tiled=True),
-        gate_cols,
-        up_cols,
+        ring_gather(arrived.reshape(ep_count * capacity, model_width), "tp", 0), gate_cols, up_cols
     )
     mixed_sum = lax.psum_scatter(
         jnp.dot(attended, out_weight, preferred_element_type=jnp.float32).astype(jnp.bfloat16),

time: 592 us -> 548 us (0.926)
  waiting for transfers between devices: 270 us -> 203 us
  blocking collectives: 63.4 us -> 76.6 us
  local copies, waits for them, and re-layouts: 43.9 us -> 53.2 us
    all_gather x1, waiting for transfers between devices: 66.6 us -> 0.02 us  [in_one_piece(): filled, at, done = (lax.all_gather(both, axis, axis=dim, tiled=True), 0, [])]
    ppermute x0 -> x3, waiting for transfers between devices: none -> 43.5 us  [the longest x2 43.5 us: ring_gather(): from_left = lax.ppermute(from_left, axis, forward)]
    all_gather x1 -> x0, waiting for transfers between devices: 41 us -> none  [body(): lax.all_gather(arrived.reshape(ep_count * capacity, model_width), 'tp', a...]
    all_to_all x1, waiting for transfers between devices: 39.7 us -> 0.01 us  [body(): lax.all_to_all(expert_sum.astype(jnp.bfloat16).reshape(ep_count, capacity...]
    ppermute x12, waiting for transfers between devices: 36.2 us -> 74.7 us  [partner(): return lax.ppermute(value, axis, pairs)]
    all_to_all x1, blocking collectives: 63.4 us -> 76.6 us  [body(): lax.all_to_all(outbound, 'ep', split_axis=0, concat_axis=0, tiled=True)]
  transfers between devices with their start and end apart: 17 -> 19, of which waited for: 14 -> 13; matrix products, arithmetic and copies ran while one was open for 33% -> 40% of each run, Pallas kernels for 0% -> 0%
where the time goes in v1:
time: 548 us; the launch traced here: 537 us
  waiting for transfers between devices  203 us (37%)
  other arithmetic  90.4 us (16%)
  blocking collectives  76.6 us (14%)
  matrix products  74.1 us (14%)
  local copies, waits for them, and re-layouts  53.2 us (10%)
  starting transfers between devices  23.8 us (4%)
  between operations  14.6 us (3%)
    reduce_scatter x1, waiting for transfers between devices, body(): lax.psum_scatter(jnp.dot(attended, out_weight, preferred_element_type=jnp...  84.5 us
    all_to_all x1, blocking collectives, body(): lax.all_to_all(outbound, 'ep', split_axis=0, concat_axis=0, tiled=True)  76.6 us
    ppermute x12, waiting for transfers between devices, partner(): return lax.ppermute(value, axis, pairs)  74.7 us
    another operation x36, other arithmetic  44.3 us
    ppermute x2, waiting for transfers between devices, ring_gather(): from_left = lax.ppermute(from_left, axis, forward)  43.5 us
    dot_general x17, matrix products, visit(): jnp.einsum('rkgd,skd->kgrs', query_rows, key_tile_rows, preferred_element...  32.2 us
    convert_element_type x17, other arithmetic, visit(): weights = jnp.where(earlier, jnp.exp(jax.nn.log_sigmoid(scores) + after +...  26.1 us
    dot_general x17, matrix products, visit(): jnp.einsum('kgrs,skd->kgrd', weights, value_block, preferred_element_type...  22.1 us
  transfers between devices with their start and end apart: 19, of which 13 were waited for; matrix products, arithmetic and copies ran while one was open for 40% of the time, Pallas kernels for 0%

profile of v1, /device:TPU:8, one launch (start us, length us, event | category | flops | bytes accessed | tf_op | source)
XLA Modules:
  0.0 537.5 jit_solution(13042074682978981185)
XLA Ops:
  17.8 4.1 scatter_custom_fusion
  22.0 3.7 reshape.326
  25.7 76.6 %all_to_all.15 = bf16[64,6,2048]{2,1,0:T(8,128)(2,1)} all-to-all(bf16[64,6,2048]{2,1,0:T(8,128)(2,1)} %reshape.326), channel_id=1, replica_groups=mesh['ep'=64,'tp'=4] {'ep'}, dimensions={0} | all-to-all | bytes 3145728 | tf_op jit(solution)/shard_map/all_to_all | solution.py:176
  102.3 3.8 reshape.327
  109.3 34.0 %collective-permute-done.12 = bf16[384,2048]{1,0:T(8,128)(2,1)} collective-permute-done((bf16[384,2048]{1,0:T(8,128)(2,1)}, bf16[384,2048]{1,0:T(8,128)(2,1)}, u32[]{:S(2)}, u32[]{:S(2)}) %collective-permute-start.12) | collective-permute-done | bytes 1572896 | tf_op jit(solution)/shard_map/ppermute | solution.py:17
  144.8 4.3 collective-permute-done.1
  150.8 4.1 collective-permute-done.2
  154.9 4.3 collective-permute-done.3
  159.1 5.3 collective-permute-done.4
  170.2 9.5 %collective-permute-done.14 = bf16[384,2048]{1,0:T(8,128)(2,1)} collective-permute-done((bf16[384,2048]{1,0:T(8,128)(2,1)}, bf16[384,2048]{1,0:T(8,128)(2,1)}, u32[]{:S(2)}, u32[]{:S(2)}) %collective-permute-start.14) | collective-permute-done | bytes 1572896 | tf_op jit(solution)/shard_map/ppermute | solution.py:17
  181.3 2.6 copy-done.2
  183.9 5.3 fusion.55
  189.2 11.8 %convolution_convert_fusion = bf16[1536,2048]{1,0:T(8,128)(2,1)} fusion(bf16[1,512,2048]{2,1,0:T(8,128)(2,1)S(1)} %copy-done, f32[1536,512]{1,0:T(8,128)} %fusion.55, bf16[1536,2048]{1,0:T(8,128)(2,1)} %copy-done.2, bf16[1,2048,512]{2,1,0:T(8,128)(2,1)} %param.24), kind=kOutput, calls=%fused_computation.74 | convolution fusion | flops 6450315264 | bytes 19922944 | tf_op jit(solution)/shard_map/dot_general | solution.py:187
  201.1 5.2 all-to-all-start.1
  206.3 5.7 %slice_bitcast_fusion.4 = (bf16[16384,1,128]{2,0,1:T(8,128)(2,1)}, bf16[16384,1,128]{2,0,1:T(8,128)(2,1)}) fusion(bf16[16384,258]{1,0:T(8,128)(2,1)} %all-gather.2.cloned.1.call-done), kind=kLoop, calls=%fused_computation.75 | loop fusion | bytes 16777216 | tf_op jit(solution)/shard_map/reshape | solution.py:33
  212.0 3.8 slice.59
  215.8 3.7 copy.53
  219.6 125.7 %while.31 = (s32[]{:T(128)}, f32[1,2,128,128]{3,2,1,0:T(8,128)S(1)}, f32[1,2,128]{2,1,0:T(2,128)S(1)}, s32[]{:T(128)}, s32[]{:T(128)}, /*index=5*/bf16[16384,1,1...) while((s32[]{:T(128)}, ...), condition=%wide.region_9.10_spmd.clone, body=%wide.region_5.9_spmd.clone.sunk | while | flops 176343936 | bytes 10775783 | solution.py:113
  220.1 1.9 fusion.101
  222.0 2.5 fusion.102
  227.9 1.9 fusion.101
  229.8 2.5 fusion.102
  235.8 1.9 fusion.101
  237.6 2.5 fusion.102
  243.6 1.9 fusion.101
  245.5 2.5 fusion.102
  251.4 1.9 fusion.101
  253.3 2.5 fusion.102
  259.3 1.9 fusion.101
  261.2 2.5 fusion.102
  267.1 1.9 fusion.101
  269.0 2.5 fusion.102
  275.0 1.9 fusion.101
  276.9 2.5 fusion.102
  282.8 1.9 fusion.101
  284.7 2.5 fusion.102
  290.7 1.9 fusion.101
  292.6 2.5 fusion.102
  298.5 1.9 fusion.101
  300.4 2.5 fusion.102
  306.3 1.9 fusion.101
  308.2 2.5 fusion.102
  314.2 1.9 fusion.101
  316.1 2.5 fusion.102
  322.0 1.9 fusion.101
  323.9 2.5 fusion.102
  329.9 1.9 fusion.101
  331.8 2.5 fusion.102
  337.7 1.9 fusion.101
  339.6 2.5 fusion.102
  346.8 4.3 collective-permute-done.7
  351.0 5.8 %collective-permute-done.8 = bf16[128,256]{0,1:T(8,128)(2,1)S(1)} collective-permute-done((bf16[128,256]{0,1:T(8,128)(2,1)S(1)}, bf16[128,256]{0,1:T(8,128)(2,1)S(1)}, u32[]{:S(2)}, u32[]{:S(2)}) %collective-permute-start.8) | collective-permute-done | bytes 65568 | tf_op jit(solution)/shard_map/ppermute | solution.py:41
  356.8 4.3 collective-permute-done.9
  361.1 4.2 reduce_sum.69
  366.9 6.4 %all-to-all-start.2 = ((bf16[64,6,2048]{2,1,0:T(8,128)(2,1)}), bf16[64,6,2048]{2,1,0:T(8,128)(2,1)}, u32[]{:S(2)}, u32[]{:S(2)}) async-start(bf16[64,6,2048]{2,1,0:T(8,128)(2,1)} %reshape.329), calls=%async_computation.3 | async-start | bytes 4194304 | tf_op jit(solution)/shard_map/all_to_all | solution.py:189
  373.3 5.6 %collective-permute-start.11 = (bf16[128,256]{0,1:T(8,128)(2,1)S(1)}, bf16[128,256]{0,1:T(8,128)(2,1)S(1)}, u32[]{:S(2)}, u32[]{:S(2)}) collective-permute-start(bf16[128,256]{0,1:T(8,128)(2,1)S(1)} %collective-permute-done.10), channel_id=1, source_target_pairs={{0,128},{4,132},{8,136},{12,140},{16,144},{20,148},{24,152},{28,15... | collective-permute-start | bytes 196616 | tf_op jit(solution)/shard_map/ppermute | solution.py:41
  378.9 8.1 %while.30 = (s32[]{:T(128)}, f32[1,2,128,128]{3,2,1,0:T(8,128)S(1)}, f32[1,2,128]{2,1,0:T(2,128)S(1)}, s32[]{:T(128)}, s32[]{:T(128)}, /*index=5*/bf16[16384,1,1...) while((s32[]{:T(128)}, ...), condition=%wide.region_4.5_spmd.clone, body=%wide.region_0.4_spmd.clone.sunk | while | flops 176343936 | bytes 10775783 | solution.py:113
  381.3 2.5 fusion.95
  387.1 40.0 %collective-permute-done.11 = bf16[128,256]{0,1:T(8,128)(2,1)S(1)} collective-permute-done((bf16[128,256]{0,1:T(8,128)(2,1)S(1)}, bf16[128,256]{0,1:T(8,128)(2,1)S(1)}, u32[]{:S(2)}, u32[]{:S(2)}) %collective-permute-start.11) | collective-permute-done | bytes 65568 | tf_op jit(solution)/shard_map/ppermute | solution.py:41
  427.1 2.7 convolution_convert_fusion.1
  430.3 3.7 reshape.330
  434.1 4.1 gather_fusion
  439.7 6.2 %multiply_reduce_fusion = bf16[128,2048]{1,0:T(8,128)(2,1)} fusion(bf16[128,2,2048]{2,1,0:T(2,128)(2,1)} %gather.7, pred[128,2]{1,0:T(8,128)(4,1)S(1)} %copy.62, f32[128,2]{1,0:T(8,128)S(1)} %copy.64), kind=kLoop, calls=%fused_computation.84 | loop fusion | flops 1835008 | bytes 1574144 | tf_op jit(solution)/shard_map/reduce_sum | solution.py:200
  445.9 84.5 %reduce-scatter.2.cloned.1.call-done = bf16[64,2048]{1,0:T(8,128)(2,1)} async-done(((bf16[256,2048]{1,0:T(8,128)(2,1)}), bf16[64,2048]{1,0:T(8,128)(2,1)}) %reduce-scatter.2.cloned.1.call-update) | async-done | bytes 262160 | tf_op jit(solution)/shard_map/reduce_scatter | solution.py:180
  (272 shorter events, 87.8 us)
Async XLA Ops:
  7.2 182.1 %copy-start = (bf16[1,512,2048]{2,1,0:T(8,128)(2,1)S(1)}, bf16[1,512,2048]{2,1,0:T(8,128)(2,1)}, u32[]{:S(2)}) copy-start(bf16[1,512,2048]{2,1,0:T(8,128)(2,1)} %param.25) | copy-start | bytes 6291460
  7.2 199.2 %all-gather.2.cloned.1.call-start = ((), (), s32[]{:S(2)}) async-start(), calls=%async_computation.4 | async-start | bytes 12779520 | tf_op jit(solution)/shard_map/all_gather | solution.py:30
  25.7 117.7 %copy-start.4 = (bf16[256,2,128]{2,1,0:T(2,128)(2,1)S(1)}, bf16[256,2,128]{2,1,0:T(2,128)(2,1)}, u32[]{:S(2)}) copy-start(bf16[256,2,128]{2,1,0:T(2,128)(2,1)} %param.16) | copy-start | bytes 393220
  106.1 37.2 %collective-permute-start.12 = (bf16[384,2048]{1,0:T(8,128)(2,1)}, bf16[384,2048]{1,0:T(8,128)(2,1)}, u32[]{:S(2)}, u32[]{:S(2)}) collective-permute-start(bf16[384,2048]{1,0:T(8,128)(2,1)} %reshape.327), channel_id=1, source_target_pairs={{0,1},{1,2},{2,3},{3,0},{4,5},{5,6},{6,7},{7,4},{8,9},{9,10},{10,1... | collective-permute-start | bytes 4718600 | tf_op jit(solution)/shard_map/ppermute | solution.py:17
  107.6 60.9 %collective-permute-start.13 = (bf16[384,2048]{1,0:T(8,128)(2,1)}, bf16[384,2048]{1,0:T(8,128)(2,1)}, u32[]{:S(2)}, u32[]{:S(2)}) collective-permute-start(bf16[384,2048]{1,0:T(8,128)(2,1)} %reshape.327), channel_id=1, source_target_pairs={{0,3},{1,0},{2,1},{3,2},{4,7},{5,4},{6,5},{7,6},{8,11},{9,8},{10,9... | collective-permute-start | bytes 4718600 | tf_op jit(solution)/shard_map/ppermute | solution.py:20
  143.3 36.4 %collective-permute-start.14 = (bf16[384,2048]{1,0:T(8,128)(2,1)}, bf16[384,2048]{1,0:T(8,128)(2,1)}, u32[]{:S(2)}, u32[]{:S(2)}) collective-permute-start(bf16[384,2048]{1,0:T(8,128)(2,1)} %collective-permute-done.12), channel_id=1, source_target_pairs={{0,1},{1,2},{2,3},{3,0},{4,5},{5,6},{6,7},{7,4},{8,9},{9,10},{10,1... | collective-permute-start | bytes 4718600 | tf_op jit(solution)/shard_map/ppermute | solution.py:17
  143.5 1.3 collective-permute-start
  144.8 4.3 collective-permute-start.1
  149.1 5.8 %collective-permute-start.2 = (bf16[128,2,128]{2,0,1:T(8,128)(2,1)S(1)}, bf16[128,2,128]{2,0,1:T(8,128)(2,1)S(1)}, u32[]{:S(2)}, u32[]{:S(2)}) collective-permute-start(bf16[128,2,128]{2,0,1:T(8,128)(2,1)S(1)} %collective-permute-done.1), channel_id=1, source_target_pairs={{0,16},{4,20},{8,24},{12,28},{16,0},{20,4},{24,8},{28,12},{32,48},... | collective-permute-start | bytes 196616 | tf_op jit(solution)/shard_map/ppermute | solution.py:41
  154.9 4.3 collective-permute-start.3
  159.1 5.3 collective-permute-start.4
  159.1 7.5 %copy-start.3 = (bf16[384,2048]{1,0:T(8,128)(2,1)S(1)}, bf16[384,2048]{1,0:T(8,128)(2,1)}, u32[]{:S(2)}) copy-start(bf16[384,2048]{1,0:T(8,128)(2,1)} %reshape.327) | copy-start | bytes 4718596
  164.4 55.1 %collective-permute-start.5 = (bf16[128,2,128]{2,0,1:T(8,128)(2,1)S(1)}, bf16[128,2,128]{2,0,1:T(8,128)(2,1)S(1)}, u32[]{:S(2)}, u32[]{:S(2)}) collective-permute-start(bf16[128,2,128]{2,0,1:T(8,128)(2,1)S(1)} %collective-permute-done.4), channel_id=1, source_target_pairs={{0,128},{4,132},{8,136},{12,140},{16,144},{20,148},{24,152},{28,15... | collective-permute-start | bytes 196616 | tf_op jit(solution)/shard_map/ppermute | solution.py:41
  168.4 15.5 %copy-start.7 = (bf16[1,2048,512]{2,1,0:T(8,128)(2,1)S(1)}, bf16[1,2048,512]{2,1,0:T(8,128)(2,1)}, u32[]{:S(2)}) copy-start(bf16[1,2048,512]{2,1,0:T(8,128)(2,1)} %param.23) | copy-start | bytes 6291460
  181.3 2.6 copy-start.2
  201.1 160.0 %all-to-all-start.1 = ((bf16[4,384,2048]{2,1,0:T(8,128)(2,1)}), bf16[4,384,2048]{2,1,0:T(8,128)(2,1)}, u32[]{:S(2)}, u32[]{:S(2)}) async-start(bf16[4,384,2048]{2,1,0:T(8,128)(2,1)} %bitcast.214), calls=%async_computation.2 | async-start | bytes 12582912 | tf_op jit(solution)/shard_map/all_to_all | solution.py:51
  345.4 1.3 collective-permute-start.6
  346.8 4.3 collective-permute-start.7
  351.0 5.8 %collective-permute-start.8 = (bf16[128,256]{0,1:T(8,128)(2,1)S(1)}, bf16[128,256]{0,1:T(8,128)(2,1)S(1)}, u32[]{:S(2)}, u32[]{:S(2)}) collective-permute-start(bf16[128,256]{0,1:T(8,128)(2,1)S(1)} %collective-permute-done.7), channel_id=1, source_target_pairs={{0,16},{4,20},{8,24},{12,28},{16,0},{20,4},{24,8},{28,12},{32,48},... | collective-permute-start | bytes 196616 | tf_op jit(solution)/shard_map/ppermute | solution.py:41
  356.8 4.3 collective-permute-start.9
  361.1 12.3 %collective-permute-start.10 = (bf16[128,256]{0,1:T(8,128)(2,1)S(1)}, bf16[128,256]{0,1:T(8,128)(2,1)S(1)}, u32[]{:S(2)}, u32[]{:S(2)}) collective-permute-start(bf16[128,256]{0,1:T(8,128)(2,1)S(1)} %collective-permute-done.9), channel_id=1, source_target_pairs={{0,64},{4,68},{8,72},{12,76},{16,80},{20,84},{24,88},{28,92},{32,9... | collective-permute-start | bytes 196616 | tf_op jit(solution)/shard_map/ppermute | solution.py:41
  366.9 63.5 %all-to-all-start.2 = ((bf16[64,6,2048]{2,1,0:T(8,128)(2,1)}), bf16[64,6,2048]{2,1,0:T(8,128)(2,1)}, u32[]{:S(2)}, u32[]{:S(2)}) async-start(bf16[64,6,2048]{2,1,0:T(8,128)(2,1)} %reshape.329), calls=%async_computation.3 | async-start | bytes 4194304 | tf_op jit(solution)/shard_map/all_to_all | solution.py:189
  373.3 157.1 %reduce-scatter.2.cloned.1.call-start = ((), (), s32[]{:S(2)}) async-start(), calls=%async_computation.5 | async-start | bytes 1310720 | tf_op jit(solution)/shard_map/reduce_scatter | solution.py:180
  373.3 53.8 %collective-permute-start.11 = (bf16[128,256]{0,1:T(8,128)(2,1)S(1)}, bf16[128,256]{0,1:T(8,128)(2,1)S(1)}, u32[]{:S(2)}, u32[]{:S(2)}) collective-permute-start(bf16[128,256]{0,1:T(8,128)(2,1)S(1)} %collective-permute-done.10), channel_id=1, source_target_pairs={{0,128},{4,132},{8,136},{12,140},{16,144},{20,148},{24,152},{28,15... | collective-permute-start | bytes 196616 | tf_op jit(solution)/shard_map/ppermute | solution.py:41
  387.0 43.0 %copy-start.5 = (s32[128,2]{0,1:T(2,128)S(1)}, s32[128,2]{0,1:T(2,128)}, u32[]{:S(2)}) copy-start(s32[128,2]{0,1:T(2,128)} %param.26) | copy-start | bytes 3076
  387.0 43.2 %copy-start.6 = (f32[128,2]{0,1:T(2,128)S(1)}, f32[128,2]{0,1:T(2,128)}, u32[]{:S(2)}) copy-start(f32[128,2]{0,1:T(2,128)} %param.27) | copy-start | bytes 3076
  434.1 96.4 %copy-start.1 = (bf16[1,512,2048]{2,1,0:T(8,128)(2,1)S(1)}, bf16[1,512,2048]{2,1,0:T(8,128)(2,1)}, u32[]{:S(2)}) copy-start(bf16[1,512,2048]{2,1,0:T(8,128)(2,1)} %param.25) | copy-start | bytes 6291460
Sparse Core Ops, SparseCore 0:
  11.3 110.3 all-gather.1
  429.9 100.4 reduce-scatter.1
